TPU v7x, 32 devices: a whole 2x2x4 slice. The times are simulated.
32 devices in a mesh: sp: 8 (over z, x), tp: 4 (over y, core).
Axes of the slice: x: 2, y: 2, z: 4, core: 2. Of those that a mesh axis runs over, the one named last changes fastest.
Arguments:
- tokens: bfloat16 [6144, 4096], P('sp', 'tp'), may hold values from -6 to 6
- norm_gain: float32 [4096], replicated, may hold values from 0.1 to 1.9
- w_query: bfloat16 [4096, 2048], P('sp', 'tp'), may hold values from -0.09375 to 0.09375
- w_key: bfloat16 [4096, 1024], P('sp', 'tp'), may hold values from -0.09375 to 0.09375
- w_value: bfloat16 [4096, 1024], P('sp', 'tp'), may hold values from -0.09375 to 0.09375
- w_pool: bfloat16 [4096, 1024], P('sp', 'tp'), may hold values from -0.09375 to 0.09375
- query_gain: float32 [64], replicated, may hold values from 0.5 to 8
- key_gain: float32 [64], replicated, may hold values from 0.5 to 8
- sink_logit: float32 [32], P('tp'), may hold values from 1 to 5
- w_out_pool: bfloat16 [1024, 4096], P('tp', 'sp'), may hold values from -0.75 to 0.75
- w_out_attn: bfloat16 [2048, 4096], P('tp', 'sp'), may hold values from -1.5 to 1.5
Outputs:
- mixed: bfloat16 [6144, 4096], P(('sp', 'tp'))
All inputs are finite; a program needn't handle non-finite values.
Results may differ from a plain program's by a relative error of at most 0.014.
The roundings to bfloat16 on the way count: a program that leaves them out, or rounds other values in their place, can miss the bound.
Values may be sent and summed in bfloat16 or wider, within the bound.
A program may use at most 128 MiB of HBM per device.

v0:
```python
import jax
import jax.numpy as jnp
from jax import lax
from jax.sharding import PartitionSpec as P

HEAD = 64
POOL = 1024
WINDOW = 128
GRID_W = 64
eps = 1e-06
rope_base = 10000.0
neg_big = -1e30
pool_reach = 8


def padded_2(block, sides, width):
    for axis, dim in sides:
        count = lax.axis_size(axis)
        forward = [(i, i + 1) for i in range(count - 1)]
        backward = [(target, source) for source, target in forward]
        low = lax.ppermute(
            lax.slice_in_dim(block, block.shape[dim] - width, None, axis=dim), axis, forward
        )
        high = lax.ppermute(lax.slice_in_dim(block, 0, width, axis=dim), axis, backward)
        block = jnp.concatenate([low, block, high], axis=dim)
    return block


def rope_tables(positions, head_size):
    quarter = head_size // 4
    freqs = 1.0 / rope_base ** (jnp.arange(quarter, dtype=jnp.float32) * 2.0 / (head_size // 2))
    row_angle = (positions // GRID_W).astype(jnp.float32)[:, None] * freqs
    col_angle = (positions % GRID_W).astype(jnp.float32)[:, None] * freqs
    angles = jnp.concatenate([row_angle, row_angle, col_angle, col_angle], axis=-1)
    return (jnp.cos(angles), jnp.sin(angles))


def rotate(heads_in, cosine, sine):
    part_one, part_two, part_three, part_four = jnp.split(heads_in, 4, axis=-1)
    turned = jnp.concatenate([-part_two, part_one, -part_four, part_three], axis=-1)
    return heads_in * cosine[:, None, :] + turned * sine[:, None, :]


def prepare(projected, gain, cosine, sine):
    rows_count = projected.shape[0]
    shaped = projected.reshape(rows_count, -1, HEAD)
    scaled = shaped * lax.rsqrt(jnp.mean(shaped * shaped, axis=-1, keepdims=True) + eps) * gain
    return rotate(scaled, cosine, sine).reshape(rows_count, -1).astype(jnp.bfloat16)


def edge_keys(keys_new, values_new):
    joined = jnp.concatenate([keys_new, values_new], axis=1)
    return padded_2(joined, (("sp", 0),), WINDOW)


def edge_pool(pool_in):
    return padded_2(pool_in, (("sp", 0),), pool_reach)


def window_attention(queries, key_band, sink_logit, positions, seq):
    rows_count = queries.shape[0]
    key_width = key_band.shape[1] // 2
    heads_q = queries.shape[1] // HEAD
    heads_k = key_width // HEAD
    group = heads_q // heads_k
    blocks = rows_count // WINDOW
    stacked = key_band.reshape(blocks + 2, WINDOW, 2 * key_width)
    joined = jnp.concatenate([stacked[:-2], stacked[1:-1], stacked[2:]], axis=1)
    block_keys = joined[:, :, :key_width].reshape(blocks, 3 * WINDOW, heads_k, HEAD)
    block_values = joined[:, :, key_width:].reshape(blocks, 3 * WINDOW, heads_k, HEAD)
    block_queries = queries.reshape(blocks, WINDOW, heads_k, group, HEAD)
    scores = jnp.einsum(
        "nqhgd,nkhd->nhgqk", block_queries, block_keys, preferred_element_type=jnp.float32
    ) * HEAD ** (-0.5)
    query_pos = positions.reshape(blocks, WINDOW)
    key_pos = query_pos[:, :1] - WINDOW + jnp.arange(3 * WINDOW, dtype=jnp.int32)[None, :]
    inside = (
        (jnp.abs(query_pos[:, :, None] - key_pos[:, None, :]) <= WINDOW)
        & (key_pos[:, None, :] >= 0)
        & (key_pos[:, None, :] < seq)
    )
    scores = jnp.where(inside[:, None, None], scores, neg_big)
    sink = sink_logit.reshape(heads_k, group)[None, :, :, None, None]
    top = jnp.maximum(jnp.max(scores, axis=-1, keepdims=True), sink)
    raised = jnp.exp(scores - top)
    totals = jnp.sum(raised, axis=-1, keepdims=True) + jnp.exp(sink - top)
    weights = (raised / totals).astype(jnp.bfloat16)
    result = jnp.einsum(
        "nhgqk,nkhd->nqhgd", weights, block_values, preferred_element_type=jnp.float32
    )
    return result.astype(jnp.bfloat16).reshape(rows_count, heads_q * HEAD)


def window_pool(pool_band, pool_in, positions, seq):
    rows_count = pool_in.shape[0]
    level = lax.axis_index("tp") * pool_in.shape[1] // (POOL // 4)
    padded = pool_band.astype(jnp.float32)
    sum_two = padded[:-1] + padded[1:]
    sum_four = sum_two[:-2] + sum_two[2:]
    sum_eight = sum_four[:-4] + sum_four[4:]
    sum_sixteen = sum_eight[:-8] + sum_eight[8:]
    candidates = jnp.stack(
        [
            sum_two[7 : 7 + rows_count],
            sum_four[6 : 6 + rows_count],
            sum_eight[4 : 4 + rows_count],
            sum_sixteen[:rows_count],
        ]
    )
    chosen = lax.dynamic_index_in_dim(candidates, level, 0, keepdims=False)
    reach = jnp.left_shift(jnp.int32(1), level)
    low = jnp.clip(positions - reach, 0, seq - 1)
    high = jnp.clip(positions + reach - 1, 0, seq - 1)
    counted = (high - low + 1).astype(jnp.float32)
    return (chosen / counted[:, None]).astype(jnp.bfloat16)


def shards(
    tokens,
    norm_gain,
    w_query,
    w_key,
    w_value,
    w_pool,
    query_gain,
    key_gain,
    sink_logit,
    w_out_pool,
    w_out_attn,
):
    gathered = lax.all_gather(tokens, "tp", axis=1, tiled=True)
    rows_count = gathered.shape[0]
    widened = gathered.astype(jnp.float32)
    normed = (
        widened * lax.rsqrt(jnp.mean(widened * widened, axis=1, keepdims=True) + eps) * norm_gain
    ).astype(jnp.bfloat16)
    positions = lax.axis_index("sp") * rows_count + jnp.arange(rows_count, dtype=jnp.int32)
    seq = lax.axis_size("sp") * rows_count
    cosine, sine = rope_tables(positions, HEAD)
    pieces = (
        lax.all_gather(w_query, "sp", axis=0, tiled=True),
        lax.all_gather(w_key, "sp", axis=0, tiled=True),
        lax.all_gather(w_value, "sp", axis=0, tiled=True),
        lax.all_gather(w_pool, "sp", axis=0, tiled=True),
    )
    query_raw, key_raw, value_raw, pool_raw = tuple(
        (jnp.dot(normed, piece, preferred_element_type=jnp.float32) for piece in pieces)
    )
    queries = prepare(query_raw, query_gain, cosine, sine)
    keys_new = prepare(key_raw, key_gain, cosine, sine)
    pool_in = pool_raw.astype(jnp.bfloat16)
    key_band = edge_keys(keys_new, value_raw.astype(jnp.bfloat16))
    pool_band = edge_pool(pool_in)
    pooled = window_pool(pool_band, pool_in, positions, seq)
    attended = window_attention(queries, key_band, sink_logit, positions, seq)
    out_pool, out_attn = (
        lax.all_gather(w_out_pool, "sp", axis=1, tiled=True),
        lax.all_gather(w_out_attn, "sp", axis=1, tiled=True),
    )
    return lax.psum_scatter(
        (
            jnp.dot(pooled, out_pool, preferred_element_type=jnp.float32)
            + jnp.dot(attended, out_attn, preferred_element_type=jnp.float32)
        ).astype(jnp.bfloat16),
        "tp",
        scatter_dimension=0,
        tiled=True,
    )


def solution(mesh):
    placed = (
        P("sp", "tp"),
        P(),
        P("sp", "tp"),
        P("sp", "tp"),
        P("sp", "tp"),
        P("sp", "tp"),
        P(),
        P(),
        P("tp"),
        P("tp", "sp"),
        P("tp", "sp"),
    )
    return jax.shard_map(
        shards, mesh=mesh, in_specs=placed, out_specs=P(("sp", "tp"), None), check_vma=False
    )
```

profile of v0, /device:TPU:0, one launch (start us, length us, event | category | flops | bytes accessed | tf_op | source)
XLA Modules:
  0.0 483.8 jit_solution(7171826045617975616)
XLA Ops:
  12.3 2.8 fusion.11
  15.1 42.9 %all-gather.8.cloned.1.call-done = bf16[768,4096]{1,0:T(8,128)(2,1)} async-done(((bf16[768,1024]{1,0:T(8,128)(2,1)}), bf16[768,4096]{1,0:T(8,128)(2,1)}) %all-gather.8.cloned.1.call-update) | async-done | bytes 6291472 | tf_op jit(solution)/shard_map/all_gather | solution.py:131
  58.0 4.2 fusion
  62.6 5.3 %fusion.2 = bf16[768,4096]{1,0:T(8,128)(2,1)} fusion(bf16[768,4096]{1,0:T(8,128)(2,1)S(1)} %copy-done, f32[4096]{0:T(1024)S(1)} %copy-done.12, f32[768]{0:T(1024)S(1)} %add_rsqrt_fusion.2), kind=kLoop, calls=%fused_computation.4 | loop fusion | flops 12582912 | bytes 12602368 | tf_op jit(solution)/shard_map/convert_element_type | solution.py:136
  68.0 41.3 %all-gather.14.cloned.1.call-done = bf16[4096,256]{1,0:T(8,128)(2,1)} async-done(((bf16[512,256]{1,0:T(8,128)(2,1)}), bf16[4096,256]{1,0:T(8,128)(2,1)}) %all-gather.14.cloned.1.call-update) | async-done | bytes 2097168 | tf_op jit(solution)/shard_map/all_gather | solution.py:142
  109.3 5.3 %multiply_reduce_fusion.1 = (f32[768,4]{0,1:T(4,128)S(1)}, f32[768,256]{0,1:T(8,128)S(1)}) fusion(bf16[768,4096]{1,0:T(8,128)(2,1)} %fusion.2, bf16[4096,256]{1,0:T(8,128)(2,1)} %all-gather.14.cloned.1.call-done), kind=kOutput, calls=%fused_computation.66 | convolution fusion | flops 1611002880 | bytes 9187328 | tf_op jit(solution)/shard_map/dot_general | solution.py:147
  115.0 44.0 %all-gather.16.cloned.1.call-done = bf16[4096,256]{1,0:T(8,128)(2,1)} async-done(((bf16[512,256]{1,0:T(8,128)(2,1)}), bf16[4096,256]{1,0:T(8,128)(2,1)}) %all-gather.16.cloned.1.call-update) | async-done | bytes 2097168 | tf_op jit(solution)/shard_map/all_gather | solution.py:143
  159.0 5.2 %convolution_convert_fusion = bf16[768,256]{0,1:T(8,128)(2,1)S(1)} fusion(bf16[768,4096]{1,0:T(8,128)(2,1)} %fusion.2, bf16[4096,256]{1,0:T(8,128)(2,1)} %all-gather.16.cloned.1.call-done), kind=kOutput, calls=%fused_computation.27 | convolution fusion | flops 1610809344 | bytes 8781824 | tf_op jit(solution)/shard_map/dot_general | solution.py:147
  165.0 3.1 collective-permute-start.2
  168.1 1.5 collective-permute-start.3
  169.6 64.8 %all-gather.18.cloned.1.call-done = bf16[4096,512]{1,0:T(8,128)(2,1)} async-done(((bf16[512,512]{1,0:T(8,128)(2,1)}), bf16[4096,512]{1,0:T(8,128)(2,1)}) %all-gather.18.cloned.1.call-update) | async-done | bytes 4194320 | tf_op jit(solution)/shard_map/all_gather | solution.py:141
  234.4 7.1 %multiply_reduce_fusion = (f32[768,8]{0,1:T(8,128)S(1)}, f32[768,512]{0,1:T(8,128)S(1)}) fusion(bf16[768,4096]{1,0:T(8,128)(2,1)} %fusion.2, bf16[4096,512]{1,0:T(8,128)(2,1)} %all-gather.18.cloned.1.call-done), kind=kOutput, calls=%fused_computation.24 | convolution fusion | flops 3222005760 | bytes 12083200 | tf_op jit(solution)/shard_map/dot_general | solution.py:147
  242.9 41.1 %all-gather.10.cloned.1.call-done = bf16[4096,256]{1,0:T(8,128)(2,1)} async-done(((bf16[512,256]{1,0:T(8,128)(2,1)}), bf16[4096,256]{1,0:T(8,128)(2,1)}) %all-gather.10.cloned.1.call-update) | async-done | bytes 2097168 | tf_op jit(solution)/shard_map/all_gather | solution.py:144
  284.0 5.3 %convolution_convert_fusion.1 = bf16[768,256]{1,0:T(8,128)(2,1)S(1)} fusion(bf16[768,4096]{1,0:T(8,128)(2,1)} %fusion.2, bf16[4096,256]{1,0:T(8,128)(2,1)} %all-gather.10.cloned.1.call-done), kind=kOutput, calls=%fused_computation.28 | convolution fusion | flops 1610809344 | bytes 8781824 | tf_op jit(solution)/shard_map/dot_general | solution.py:147
  289.3 2.5 collective-permute-start
  291.8 1.3 collective-permute-start.1
  294.6 3.4 collective-permute-done.1
  298.4 1.3 fusion.20
  301.0 2.3 pad_maximum_fusion.4
  303.3 1.4 copy.35
  305.0 1.4 copy.34
  306.5 1.2 fusion.45
  307.8 1.7 copy.38
  309.5 1.4 copy.37
  310.9 2.7 fusion.4
  313.7 2.4 fusion.3
  316.3 2.8 fusion.9
  319.6 39.5 %all-gather.20.cloned.1.call-done = bf16[512,4096]{1,0:T(8,128)(2,1)} async-done(((bf16[512,512]{1,0:T(8,128)(2,1)}), bf16[512,4096]{1,0:T(8,128)(2,1)}) %all-gather.20.cloned.1.call-update) | async-done | bytes 4194320 | tf_op jit(solution)/shard_map/all_gather | solution.py:158
  359.1 8.9 %fusion.17 = f32[768,4096]{1,0:T(8,128)} fusion(bf16[512,4096]{1,0:T(8,128)(2,1)} %all-gather.20.cloned.1.call-done, bf16[64,8,6,128]{3,2,1,0:T(8,128)(2,1)S(1)} %bitcast.99), kind=kOutput, calls=%fused_computation.45 | convolution fusion | flops 3221225472 | bytes 17563648 | tf_op jit(solution)/shard_map/dot_general | solution.py:163
  368.0 41.7 %all-gather.12.cloned.1.call-done = bf16[256,4096]{1,0:T(8,128)(2,1)} async-done(((bf16[256,512]{1,0:T(8,128)(2,1)}), bf16[256,4096]{1,0:T(8,128)(2,1)}) %all-gather.12.cloned.1.call-update) | async-done | bytes 2097168 | tf_op jit(solution)/shard_map/all_gather | solution.py:157
  409.7 9.7 %add_convert_fusion = bf16[768,4096]{1,0:T(8,128)(2,1)} fusion(f32[768,4096]{1,0:T(8,128)} %fusion.17, bf16[256,4096]{1,0:T(8,128)(2,1)} %all-gather.12.cloned.1.call-done, s32[]{:T(128)S(6)} %select_n.33, f32[1,768,256]{2,1,0:T(8,128)S(1)} %copy-done.4, f32[1,768,256]{2,1,0:T(8,128)} %get-tuple-element.39, f32[1,768,256]{2,1,0:T(8,128)S(1)} %copy-done.2, ...), kind=kOutput, calls=%fused_computation.5 | convolution fusion | flops 1617887232 | bytes 24120324 | tf_op jit(solution)/shard_map/dot_general | solution.py:162
  419.5 57.4 %reduce-scatter.2.cloned.1.call-done = bf16[192,4096]{1,0:T(8,128)(2,1)} async-done(((bf16[768,4096]{1,0:T(8,128)(2,1)}), bf16[192,4096]{1,0:T(8,128)(2,1)}) %reduce-scatter.2.cloned.1.call-update) | async-done | bytes 1572880 | tf_op jit(solution)/shard_map/reduce_scatter | solution.py:160
  (90 shorter events, 12.8 us)
Async XLA Ops:
  6.5 5.1 %copy-start.13 = (f32[64]{0:T(128)S(1)}, f32[64]{0:T(128)}, u32[]{:S(2)}) copy-start(f32[64]{0:T(128)} %param.18) | copy-start | bytes 772
  6.5 5.2 %copy-start.14 = (f32[64]{0:T(128)S(1)}, f32[64]{0:T(128)}, u32[]{:S(2)}) copy-start(f32[64]{0:T(128)} %param.17) | copy-start | bytes 772
  6.5 5.2 %copy-start.15 = (f32[8]{0:T(128)S(1)}, f32[8]{0:T(128)}, u32[]{:S(2)}) copy-start(f32[8]{0:T(128)} %param.19) | copy-start | bytes 100
  6.5 51.5 %all-gather.8.cloned.1.call-start = ((), (), s32[]{:S(2)}) async-start(), calls=%async_computation.1 | async-start | bytes 7864320 | tf_op jit(solution)/shard_map/all_gather | solution.py:131
  7.3 102.0 %all-gather.14.cloned.1.call-start = ((), (), s32[]{:S(2)}) async-start(), calls=%async_computation.4 | async-start | bytes 2359296 | tf_op jit(solution)/shard_map/all_gather | solution.py:142
  8.0 151.0 %all-gather.16.cloned.1.call-start = ((), (), s32[]{:S(2)}) async-start(), calls=%async_computation.5 | async-start | bytes 2359296 | tf_op jit(solution)/shard_map/all_gather | solution.py:143
  8.7 225.7 %all-gather.18.cloned.1.call-start = ((), (), s32[]{:S(2)}) async-start(), calls=%async_computation.6 | async-start | bytes 4718592 | tf_op jit(solution)/shard_map/all_gather | solution.py:141
  9.3 274.7 %all-gather.10.cloned.1.call-start = ((), (), s32[]{:S(2)}) async-start(), calls=%async_computation.2 | async-start | bytes 2359296 | tf_op jit(solution)/shard_map/all_gather | solution.py:144
  9.9 349.2 %all-gather.20.cloned.1.call-start = ((), (), s32[]{:S(2)}) async-start(), calls=%async_computation.7 | async-start | bytes 4718592 | tf_op jit(solution)/shard_map/all_gather | solution.py:158
  10.5 399.2 %all-gather.12.cloned.1.call-start = ((), (), s32[]{:S(2)}) async-start(), calls=%async_computation.3 | async-start | bytes 2359296 | tf_op jit(solution)/shard_map/all_gather | solution.py:157
  11.2 465.7 %reduce-scatter.2.cloned.1.call-start = ((), (), s32[]{:S(2)}) async-start(), calls=%async_computation.8 | async-start | bytes 7864320 | tf_op jit(solution)/shard_map/reduce_scatter | solution.py:160
  12.3 49.9 %copy-start.12 = (f32[4096]{0:T(1024)S(1)}, f32[4096]{0:T(1024)}, u32[]{:S(2)}) copy-start(f32[4096]{0:T(1024)} %param.12) | copy-start | bytes 49156
  58.0 4.6 copy-start
  164.3 77.3 %copy-start.7 = (bf16[768,256]{0,1:T(8,128)(2,1)}, bf16[768,256]{0,1:T(8,128)(2,1)S(1)}, u32[]{:S(2)}) copy-start(bf16[768,256]{0,1:T(8,128)(2,1)S(1)} %convolution_convert_fusion) | copy-start | bytes 1179652
  165.0 135.9 %collective-permute-start.2 = (bf16[128,512]{0,1:T(8,128)(2,1)}, bf16[128,512]{0,1:T(8,128)(2,1)}, u32[]{:S(2)}, u32[]{:S(2)}) collective-permute-start(bf16[128,512]{0,1:T(8,128)(2,1)} %get-tuple-element.16), channel_id=1, source_target_pairs={{0,4},{4,8},{8,12},{12,16},{16,20},{20,24},{24,28},{1,5},{5,9},{9,... | collective-permute-start | bytes 393224 | tf_op jit(solution)/shard_map/ppermute | solution.py:21
  168.1 132.8 %collective-permute-start.3 = (bf16[128,512]{0,1:T(8,128)(2,1)S(1)}, bf16[128,512]{0,1:T(8,128)(2,1)}, u32[]{:S(2)}, u32[]{:S(2)}) collective-permute-start(bf16[128,512]{0,1:T(8,128)(2,1)S(1)} %get-tuple-element.17), channel_id=1, source_target_pairs={{4,0},{8,4},{12,8},{16,12},{20,16},{24,20},{28,24},{5,1},{9,5},{13... | collective-permute-start | bytes 393224 | tf_op jit(solution)/shard_map/ppermute | solution.py:24
  284.0 9.1 %copy-start.5 = (f32[768,8,16]{0,2,1:T(8,128)S(1)}, f32[768,8,16]{0,2,1:T(8,128)}, u32[]{:S(2)}) copy-start(f32[768,8,16]{0,2,1:T(8,128)} %get-tuple-element.9) | copy-start | bytes 1179652
  284.0 9.1 %copy-start.6 = (f32[768,8,16]{0,2,1:T(8,128)S(1)}, f32[768,8,16]{0,2,1:T(8,128)}, u32[]{:S(2)}) copy-start(f32[768,8,16]{0,2,1:T(8,128)} %get-tuple-element.10) | copy-start | bytes 1179652
  289.3 3.8 copy-start.10
  289.3 5.2 %collective-permute-start = (bf16[8,256]{1,0:T(8,128)(2,1)S(1)}, bf16[8,256]{1,0:T(8,128)(2,1)S(1)}, u32[]{:S(2)}, u32[]{:S(2)}) collective-permute-start(bf16[8,256]{1,0:T(8,128)(2,1)S(1)} %get-tuple-element.22), channel_id=1, source_target_pairs={{0,4},{4,8},{8,12},{12,16},{16,20},{20,24},{24,28},{1,5},{5,9},{9,... | collective-permute-start | bytes 12296 | tf_op jit(solution)/shard_map/ppermute | solution.py:21
  291.8 6.1 %collective-permute-start.1 = (bf16[8,256]{1,0:T(8,128)(2,1)S(1)}, bf16[8,256]{1,0:T(8,128)(2,1)S(1)}, u32[]{:S(2)}, u32[]{:S(2)}) collective-permute-start(bf16[8,256]{1,0:T(8,128)(2,1)S(1)} %get-tuple-element.23), channel_id=1, source_target_pairs={{4,0},{8,4},{12,8},{16,12},{20,16},{24,20},{28,24},{5,1},{9,5},{13... | collective-permute-start | bytes 12296 | tf_op jit(solution)/shard_map/ppermute | solution.py:24
  293.3 4.7 copy-start.11
  299.7 1.2 copy-start.8
  310.9 2.8 copy-start.1
  313.7 2.5 copy-start.9
  359.1 50.6 %copy-start.2 = (f32[1,768,256]{2,1,0:T(8,128)S(1)}, f32[1,768,256]{2,1,0:T(8,128)}, u32[]{:S(2)}) copy-start(f32[1,768,256]{2,1,0:T(8,128)} %get-tuple-element.40) | copy-start | bytes 2359300
  359.1 50.6 %copy-start.3 = (f32[1,768,256]{2,1,0:T(8,128)S(1)}, f32[1,768,256]{2,1,0:T(8,128)}, u32[]{:S(2)}) copy-start(f32[1,768,256]{2,1,0:T(8,128)} %get-tuple-element.41) | copy-start | bytes 2359300
  359.1 50.6 %copy-start.4 = (f32[1,768,256]{2,1,0:T(8,128)S(1)}, f32[1,768,256]{2,1,0:T(8,128)}, u32[]{:S(2)}) copy-start(f32[1,768,256]{2,1,0:T(8,128)} %get-tuple-element.38) | copy-start | bytes 2359300
Sparse Core Ops, SparseCore 0:
  8.9 49.0 all-gather.7
  60.1 49.0 all-gather.13
  111.4 47.6 all-gather.15
  161.0 73.3 all-gather.17
  236.4 47.6 all-gather.9
  285.9 73.1 all-gather.19
  361.2 48.5 all-gather.11
  419.6 57.2 reduce-scatter.1
where the time goes:
time: 484 us
  waiting for transfers between devices  381 us (79%)
  matrix products  47 us (10%)
  other arithmetic  22.8 us (5%)
  between operations  13.9 us (3%)
  local copies, waits for them, and re-layouts  10.9 us (2%)
  starting transfers between devices  8.59 us (2%)
    all_gather x1, waiting for transfers between devices, shards(): lax.all_gather(w_query, 'sp', axis=0, tiled=True)  64.8 us
    reduce_scatter x1, waiting for transfers between devices, shards(): lax.psum_scatter((jnp.dot(pooled, out_pool, preferred_element_type=jnp.fl...  57.4 us
    all_gather x1, waiting for transfers between devices, shards(): lax.all_gather(w_value, 'sp', axis=0, tiled=True)  44 us
    all_gather x1, waiting for transfers between devices, shards(): gathered = lax.all_gather(tokens, 'tp', axis=1, tiled=True)  42.9 us
    all_gather x1, waiting for transfers between devices, shards(): lax.all_gather(w_out_pool, 'sp', axis=1, tiled=True)  41.7 us
    all_gather x1, waiting for transfers between devices, shards(): lax.all_gather(w_key, 'sp', axis=0, tiled=True)  41.3 us
    all_gather x1, waiting for transfers between devices, shards(): lax.all_gather(w_pool, 'sp', axis=0, tiled=True)  41.1 us
    all_gather x1, waiting for transfers between devices, shards(): lax.all_gather(w_out_attn, 'sp', axis=1, tiled=True)  39.5 us
  transfers between devices with their start and end apart: 12, of which 9 were waited for; matrix products, arithmetic and copies ran while one was open for 15% of the time, Pallas kernels for 0%

commit v1 on v0

--- a/solution.py
+++ b/solution.py
@@ -128,7 +128,14 @@
     w_out_pool,
     w_out_attn,
 ):
-    gathered = lax.all_gather(tokens, "tp", axis=1, tiled=True)
+    dev_n = lax.axis_size("tp")
+    inter = sorted(((src_i, (src_i + 1) % dev_n) for src_i in range(dev_n)))
+    plain = tokens
+    inbox = [plain]
+    for dev_i in [*range(1, dev_n)]:
+        plain = lax.ppermute(plain, "tp", inter)
+        inbox.insert(0, plain)
+    gathered = jnp.roll(jnp.concatenate(inbox, 1), (lax.axis_index("tp") + 1) * tokens.shape[1], 1)
     rows_count = gathered.shape[0]
     widened = gathered.astype(jnp.float32)
     normed = (

time: 484 us -> 436 us (0.901)
  waiting for transfers between devices: 381 us -> 339 us
  other arithmetic: 22.8 us -> 10.8 us
    ppermute x0 -> x3, waiting for transfers between devices: none -> 54.1 us  [shards(): plain = lax.ppermute(plain, 'tp', inter)]
    all_gather x1 -> x0, waiting for transfers between devices: 42.9 us -> none  [shards(): gathered = lax.all_gather(tokens, 'tp', axis=1, tiled=True)]
    all_gather x1, waiting for transfers between devices: 41.1 us -> 0.02 us  [shards(): lax.all_gather(w_pool, 'sp', axis=0, tiled=True)]
    all_gather x1, waiting for transfers between devices: 41.3 us -> 22.8 us  [shards(): lax.all_gather(w_key, 'sp', axis=0, tiled=True)]
    all_gather x1, waiting for transfers between devices: 39.5 us -> 57 us  [shards(): lax.all_gather(w_out_attn, 'sp', axis=1, tiled=True)]
    all_gather x1, waiting for transfers between devices: 64.8 us -> 52.7 us  [shards(): lax.all_gather(w_query, 'sp', axis=0, tiled=True)]
    unnamed x32 -> x39, local copies, waits for them, and re-layouts: 0.42 us -> 6.03 us
    convert_element_type x1 -> x0, other arithmetic: 5.35 us -> none  [shards(): normed = (widened * lax.rsqrt(jnp.mean(widened * widened, axis=1, keepdim...]
  transfers between devices with their start and end apart: 12 -> 14, of which waited for: 9 -> 11; matrix products, arithmetic and copies ran while one was open for 15% -> 13% of each run, Pallas kernels for 0% -> 0%
where the time goes in v1:
time: 436 us
  waiting for transfers between devices  339 us (78%)
  matrix products  47.6 us (11%)
  local copies, waits for them, and re-layouts  14.6 us (3%)
  between operations  14 us (3%)
  other arithmetic  10.8 us (2%)
  starting transfers between devices  10.1 us (2%)
    reduce_scatter x1, waiting for transfers between devices, shards(): lax.psum_scatter((jnp.dot(pooled, out_pool, preferred_element_type=jnp.fl...  57.4 us
    all_gather x1, waiting for transfers between devices, shards(): lax.all_gather(w_out_attn, 'sp', axis=1, tiled=True)  57 us
    ppermute x3, waiting for transfers between devices, shards(): plain = lax.ppermute(plain, 'tp', inter)  54.1 us
    all_gather x1, waiting for transfers between devices, shards(): lax.all_gather(w_query, 'sp', axis=0, tiled=True)  52.7 us
    all_gather x1, waiting for transfers between devices, shards(): lax.all_gather(w_value, 'sp', axis=0, tiled=True)  43.7 us
    all_gather x1, waiting for transfers between devices, shards(): lax.all_gather(w_out_pool, 'sp', axis=1, tiled=True)  41.6 us
    dot_general x4, matrix products, shards(): jnp.dot(normed, piece, preferred_element_type=jnp.float32)  24.3 us
    all_gather x1, waiting for transfers between devices, shards(): lax.all_gather(w_key, 'sp', axis=0, tiled=True)  22.8 us
  transfers between devices with their start and end apart: 14, of which 11 were waited for; matrix products, arithmetic and copies ran while one was open for 13% of the time, Pallas kernels for 0%

profile of v1, /device:TPU:0, one launch (start us, length us, event | category | flops | bytes accessed | tf_op | source)
XLA Modules:
  0.0 435.8 jit_solution(5015718878999700573)
XLA Ops:
  10.5 20.3 %collective-permute-done = bf16[768,1024]{1,0:T(8,128)(2,1)S(1)} collective-permute-done((bf16[768,1024]{1,0:T(8,128)(2,1)}, bf16[768,1024]{1,0:T(8,128)(2,1)S(1)}, u32[]{:S(2)}, u32[]{:S(2)}) %collective-permute-start) | collective-permute-done | bytes 1572896 | tf_op jit(solution)/shard_map/ppermute | solution.py:136
  32.4 0.7 max.27
  33.1 17.5 %collective-permute-done.1 = bf16[768,1024]{1,0:T(8,128)(2,1)S(1)} collective-permute-done((bf16[768,1024]{1,0:T(8,128)(2,1)S(1)}, bf16[768,1024]{1,0:T(8,128)(2,1)S(1)}, u32[]{:S(2)}, u32[]{:S(2)}) %collective-permute-start.1) | collective-permute-done | bytes 1572896 | tf_op jit(solution)/shard_map/ppermute | solution.py:136
  51.4 2.7 fusion.11
  54.1 16.3 %collective-permute-done.2 = bf16[768,1024]{1,0:T(8,128)(2,1)S(1)} collective-permute-done((bf16[768,1024]{1,0:T(8,128)(2,1)S(1)}, bf16[768,1024]{1,0:T(8,128)(2,1)S(1)}, u32[]{:S(2)}, u32[]{:S(2)}) %collective-permute-start.2) | collective-permute-done | bytes 1572896 | tf_op jit(solution)/shard_map/ppermute | solution.py:136
  71.7 4.5 %copy-done.1 = bf16[768,8192]{1,0:T(8,128)(2,1)} copy-done((bf16[768,8192]{1,0:T(8,128)(2,1)}, bf16[768,8192]{1,0:T(8,128)(2,1)S(1)}, u32[]{:S(2)}) %copy-start.1) | copy-done | bytes 12582936
  76.2 1.3 fusion
  77.5 5.3 %convolution_convert_fusion.1 = bf16[768,256]{1,0:T(8,128)(2,1)S(1)} fusion(bf16[4096,256]{1,0:T(8,128)(2,1)} %all-gather.7.cloned.1.call-done, f32[4096]{0:T(1024)S(1)} %copy-done.15, f32[768]{0:T(1024)S(1)} %add_rsqrt_fusion.2, bf16[768,8192]{1,0:T(8,128)(2,1)} %copy-done.1, s32[]{:T(128)S(6)} %select_n.45), kind=kOutput, calls=%fused_computation.28 | convolution fusion | flops 1623392256 | bytes 8801284 | tf_op jit(solution)/shard_map/dot_general | solution.py:154
  82.8 4.2 collective-permute-start.3
  87.1 1.3 collective-permute-start.4
  88.4 22.8 %all-gather.11.cloned.1.call-done = bf16[4096,256]{1,0:T(8,128)(2,1)} async-done(((bf16[512,256]{1,0:T(8,128)(2,1)}), bf16[4096,256]{1,0:T(8,128)(2,1)}) %all-gather.11.cloned.1.call-update) | async-done | bytes 2097168 | tf_op jit(solution)/shard_map/all_gather | solution.py:149
  111.1 5.6 %multiply_reduce_fusion.1 = (f32[768,4]{0,1:T(4,128)S(1)}, f32[768,256]{0,1:T(8,128)S(1)}) fusion(bf16[4096,256]{1,0:T(8,128)(2,1)} %all-gather.11.cloned.1.call-done, f32[4096]{0:T(1024)S(1)} %copy-done.15, f32[768]{0:T(1024)S(1)} %add_rsqrt_fusion.2, bf16[768,8192]{1,0:T(8,128)(2,1)} %copy-done.1, s32[]{:T(128)S(6)} %select_n.45), kind=kOutput, calls=%fused_computation.66 | convolution fusion | flops 1623585792 | bytes 9206788 | tf_op jit(solution)/shard_map/dot_general | solution.py:154
  117.3 43.7 %all-gather.13.cloned.1.call-done = bf16[4096,256]{1,0:T(8,128)(2,1)} async-done(((bf16[512,256]{1,0:T(8,128)(2,1)}), bf16[4096,256]{1,0:T(8,128)(2,1)}) %all-gather.13.cloned.1.call-update) | async-done | bytes 2097168 | tf_op jit(solution)/shard_map/all_gather | solution.py:150
  160.9 5.6 %convolution_convert_fusion = bf16[768,256]{0,1:T(8,128)(2,1)S(1)} fusion(bf16[4096,256]{1,0:T(8,128)(2,1)} %all-gather.13.cloned.1.call-done, f32[4096]{0:T(1024)S(1)} %copy-done.15, f32[768]{0:T(1024)S(1)} %add_rsqrt_fusion.2, bf16[768,8192]{1,0:T(8,128)(2,1)} %copy-done.1, s32[]{:T(128)S(6)} %select_n.45), kind=kOutput, calls=%fused_computation.27 | convolution fusion | flops 1623392256 | bytes 8801284 | tf_op jit(solution)/shard_map/dot_general | solution.py:154
  166.6 2.5 collective-permute-start.5
  169.0 1.3 collective-permute-start.6
  170.8 1.3 fusion.20
  172.2 1.3 slice_bitcast_fusion.1
  174.0 5.7 %collective-permute-done.6 = bf16[128,512]{0,1:T(8,128)(2,1)S(1)} collective-permute-done((bf16[128,512]{0,1:T(8,128)(2,1)S(1)}, bf16[128,512]{0,1:T(8,128)(2,1)S(1)}, u32[]{:S(2)}, u32[]{:S(2)}) %collective-permute-start.6) | collective-permute-done | bytes 131104 | tf_op jit(solution)/shard_map/ppermute | solution.py:24
  181.2 0.9 copy.38
  182.1 1.4 copy.37
  183.5 52.7 %all-gather.15.cloned.1.call-done = bf16[4096,512]{1,0:T(8,128)(2,1)} async-done(((bf16[512,512]{1,0:T(8,128)(2,1)}), bf16[4096,512]{1,0:T(8,128)(2,1)}) %all-gather.15.cloned.1.call-update) | async-done | bytes 4194320 | tf_op jit(solution)/shard_map/all_gather | solution.py:148
  236.2 7.8 %multiply_reduce_fusion = (f32[768,8]{0,1:T(8,128)S(1)}, f32[768,512]{0,1:T(8,128)S(1)}) fusion(bf16[4096,512]{1,0:T(8,128)(2,1)} %all-gather.15.cloned.1.call-done, f32[4096]{0:T(1024)} %param.12, f32[768]{0:T(1024)S(1)} %copy-done.12, bf16[768,8192]{1,0:T(8,128)(2,1)} %copy-done.1, s32[]{:T(128)S(6)} %select_n.45), kind=kOutput, calls=%fused_computation.24 | convolution fusion | flops 3234588672 | bytes 12102660 | tf_op jit(solution)/shard_map/dot_general | solution.py:154
  245.5 0.9 reshape.301
  246.4 1.7 fusion.4
  248.2 2.4 fusion.3
  250.7 3.0 fusion.9
  254.3 57.0 %all-gather.17.cloned.1.call-done = bf16[512,4096]{1,0:T(8,128)(2,1)} async-done(((bf16[512,512]{1,0:T(8,128)(2,1)}), bf16[512,4096]{1,0:T(8,128)(2,1)}) %all-gather.17.cloned.1.call-update) | async-done | bytes 4194320 | tf_op jit(solution)/shard_map/all_gather | solution.py:165
  311.3 8.9 %fusion.17 = f32[768,4096]{1,0:T(8,128)} fusion(bf16[512,4096]{1,0:T(8,128)(2,1)} %all-gather.17.cloned.1.call-done, bf16[64,8,6,128]{3,2,1,0:T(8,128)(2,1)S(1)} %bitcast.95), kind=kOutput, calls=%fused_computation.45 | convolution fusion | flops 3221225472 | bytes 17563648 | tf_op jit(solution)/shard_map/dot_general | solution.py:170
  320.2 41.6 %all-gather.9.cloned.1.call-done = bf16[256,4096]{1,0:T(8,128)(2,1)} async-done(((bf16[256,512]{1,0:T(8,128)(2,1)}), bf16[256,4096]{1,0:T(8,128)(2,1)}) %all-gather.9.cloned.1.call-update) | async-done | bytes 2097168 | tf_op jit(solution)/shard_map/all_gather | solution.py:164
  361.7 9.7 %add_convert_fusion = bf16[768,4096]{1,0:T(8,128)(2,1)} fusion(f32[768,4096]{1,0:T(8,128)} %fusion.17, bf16[256,4096]{1,0:T(8,128)(2,1)} %all-gather.9.cloned.1.call-done, s32[]{:T(128)S(6)} %select_n.47, f32[1,768,256]{2,1,0:T(8,128)S(1)} %copy-done.5, f32[1,768,256]{2,1,0:T(8,128)} %get-tuple-element.39, f32[1,768,256]{2,1,0:T(8,128)S(1)} %copy-done.3, ...), kind=kOutput, calls=%fused_computation.5 | convolution fusion | flops 1617887232 | bytes 24120324 | tf_op jit(solution)/shard_map/dot_general | solution.py:169
  371.5 57.4 %reduce-scatter.2.cloned.1.call-done = bf16[192,4096]{1,0:T(8,128)(2,1)} async-done(((bf16[768,4096]{1,0:T(8,128)(2,1)}), bf16[192,4096]{1,0:T(8,128)(2,1)}) %reduce-scatter.2.cloned.1.call-update) | async-done | bytes 1572880 | tf_op jit(solution)/shard_map/reduce_scatter | solution.py:167
  (100 shorter events, 12.4 us)
Async XLA Ops:
  6.5 71.0 %all-gather.7.cloned.1.call-start = ((), (), s32[]{:S(2)}) async-start(), calls=%async_computation.1 | async-start | bytes 2359296 | tf_op jit(solution)/shard_map/all_gather | solution.py:151
  7.3 103.9 %all-gather.11.cloned.1.call-start = ((), (), s32[]{:S(2)}) async-start(), calls=%async_computation.3 | async-start | bytes 2359296 | tf_op jit(solution)/shard_map/all_gather | solution.py:149
  8.0 152.9 %all-gather.13.cloned.1.call-start = ((), (), s32[]{:S(2)}) async-start(), calls=%async_computation.4 | async-start | bytes 2359296 | tf_op jit(solution)/shard_map/all_gather | solution.py:150
  8.7 227.4 %all-gather.15.cloned.1.call-start = ((), (), s32[]{:S(2)}) async-start(), calls=%async_computation.5 | async-start | bytes 4718592 | tf_op jit(solution)/shard_map/all_gather | solution.py:148
  9.3 302.0 %all-gather.17.cloned.1.call-start = ((), (), s32[]{:S(2)}) async-start(), calls=%async_computation.6 | async-start | bytes 4718592 | tf_op jit(solution)/shard_map/all_gather | solution.py:165
  9.9 351.8 %all-gather.9.cloned.1.call-start = ((), (), s32[]{:S(2)}) async-start(), calls=%async_computation.2 | async-start | bytes 2359296 | tf_op jit(solution)/shard_map/all_gather | solution.py:164
  9.9 20.8 %collective-permute-start = (bf16[768,1024]{1,0:T(8,128)(2,1)}, bf16[768,1024]{1,0:T(8,128)(2,1)S(1)}, u32[]{:S(2)}, u32[]{:S(2)}) collective-permute-start(bf16[768,1024]{1,0:T(8,128)(2,1)} %param.11), channel_id=1, source_target_pairs={{0,1},{1,2},{2,3},{3,0},{4,5},{5,6},{6,7},{7,4},{8,9},{9,10},{10,1... | collective-permute-start | bytes 4718600 | tf_op jit(solution)/shard_map/ppermute | solution.py:136
  30.8 19.8 %collective-permute-start.1 = (bf16[768,1024]{1,0:T(8,128)(2,1)S(1)}, bf16[768,1024]{1,0:T(8,128)(2,1)S(1)}, u32[]{:S(2)}, u32[]{:S(2)}) collective-permute-start(bf16[768,1024]{1,0:T(8,128)(2,1)S(1)} %collective-permute-done), channel_id=1, source_target_pairs={{0,1},{1,2},{2,3},{3,0},{4,5},{5,6},{6,7},{7,4},{8,9},{9,10},{10,1... | collective-permute-start | bytes 4718600 | tf_op jit(solution)/shard_map/ppermute | solution.py:136
  30.8 398.1 %reduce-scatter.2.cloned.1.call-start = ((), (), s32[]{:S(2)}) async-start(), calls=%async_computation.7 | async-start | bytes 7864320 | tf_op jit(solution)/shard_map/reduce_scatter | solution.py:167
  50.6 19.8 %collective-permute-start.2 = (bf16[768,1024]{1,0:T(8,128)(2,1)S(1)}, bf16[768,1024]{1,0:T(8,128)(2,1)S(1)}, u32[]{:S(2)}, u32[]{:S(2)}) collective-permute-start(bf16[768,1024]{1,0:T(8,128)(2,1)S(1)} %collective-permute-done.1), channel_id=1, source_target_pairs={{0,1},{1,2},{2,3},{3,0},{4,5},{5,6},{6,7},{7,4},{8,9},{9,10},{10,1... | collective-permute-start | bytes 4718600 | tf_op jit(solution)/shard_map/ppermute | solution.py:136
  51.2 65.8 %copy-start.8 = (f32[768,64]{0,1:T(8,128)}, f32[768,64]{0,1:T(8,128)S(1)}, u32[]{:S(2)}) copy-start(f32[768,64]{0,1:T(8,128)S(1)} %get-tuple-element.25) | copy-start | bytes 589828
  51.2 65.9 %copy-start.6 = (f32[768,64]{0,1:T(8,128)}, f32[768,64]{0,1:T(8,128)S(1)}, u32[]{:S(2)}) copy-start(f32[768,64]{0,1:T(8,128)S(1)} %get-tuple-element.24) | copy-start | bytes 589828
  54.1 16.8 %copy-start = (bf16[768,1024]{1,0:T(8,128)(2,1)S(1)}, bf16[768,1024]{1,0:T(8,128)(2,1)}, u32[]{:S(2)}) copy-start(bf16[768,1024]{1,0:T(8,128)(2,1)} %param.11) | copy-start | bytes 4718596
  71.5 6.0 %copy-start.15 = (f32[4096]{0:T(1024)S(1)}, f32[4096]{0:T(1024)}, u32[]{:S(2)}) copy-start(f32[4096]{0:T(1024)} %param.12) | copy-start | bytes 49156
  71.7 4.5 %copy-start.1 = (bf16[768,8192]{1,0:T(8,128)(2,1)}, bf16[768,8192]{1,0:T(8,128)(2,1)S(1)}, u32[]{:S(2)}) copy-start(bf16[768,8192]{1,0:T(8,128)(2,1)S(1)} %constant_dynamic-update-slice_fusion) | copy-start | bytes 37748740
  77.5 83.5 %copy-start.11 = (f32[768]{0:T(1024)}, f32[768]{0:T(1024)S(1)}, u32[]{:S(2)}) copy-start(f32[768]{0:T(1024)S(1)} %add_rsqrt_fusion.2) | copy-start | bytes 9220
  82.8 87.5 %collective-permute-start.3 = (bf16[8,256]{1,0:T(8,128)(2,1)S(1)}, bf16[8,256]{1,0:T(8,128)(2,1)S(1)}, u32[]{:S(2)}, u32[]{:S(2)}) collective-permute-start(bf16[8,256]{1,0:T(8,128)(2,1)S(1)} %get-tuple-element.22), channel_id=1, source_target_pairs={{0,4},{4,8},{8,12},{12,16},{16,20},{20,24},{24,28},{1,5},{5,9},{9,... | collective-permute-start | bytes 12296 | tf_op jit(solution)/shard_map/ppermute | solution.py:21
  87.0 29.7 %copy-start.13 = (f32[64]{0:T(128)S(1)}, f32[64]{0:T(128)}, u32[]{:S(2)}) copy-start(f32[64]{0:T(128)} %param.18) | copy-start | bytes 772
  87.1 83.3 %collective-permute-start.4 = (bf16[8,256]{1,0:T(8,128)(2,1)S(1)}, bf16[8,256]{1,0:T(8,128)(2,1)S(1)}, u32[]{:S(2)}, u32[]{:S(2)}) collective-permute-start(bf16[8,256]{1,0:T(8,128)(2,1)S(1)} %get-tuple-element.23), channel_id=1, source_target_pairs={{4,0},{8,4},{12,8},{16,12},{20,16},{24,20},{28,24},{5,1},{9,5},{13... | collective-permute-start | bytes 12296 | tf_op jit(solution)/shard_map/ppermute | solution.py:24
  166.6 7.5 %collective-permute-start.5 = (bf16[128,512]{0,1:T(8,128)(2,1)S(1)}, bf16[128,512]{0,1:T(8,128)(2,1)S(1)}, u32[]{:S(2)}, u32[]{:S(2)}) collective-permute-start(bf16[128,512]{0,1:T(8,128)(2,1)S(1)} %get-tuple-element.16), channel_id=1, source_target_pairs={{0,4},{4,8},{8,12},{12,16},{16,20},{20,24},{24,28},{1,5},{5,9},{9,... | collective-permute-start | bytes 393224 | tf_op jit(solution)/shard_map/ppermute | solution.py:21
  169.0 10.7 %collective-permute-start.6 = (bf16[128,512]{0,1:T(8,128)(2,1)S(1)}, bf16[128,512]{0,1:T(8,128)(2,1)S(1)}, u32[]{:S(2)}, u32[]{:S(2)}) collective-permute-start(bf16[128,512]{0,1:T(8,128)(2,1)S(1)} %get-tuple-element.17), channel_id=1, source_target_pairs={{4,0},{8,4},{12,8},{16,12},{20,16},{24,20},{28,24},{5,1},{9,5},{13... | collective-permute-start | bytes 393224 | tf_op jit(solution)/shard_map/ppermute | solution.py:24
  181.0 55.2 %copy-start.12 = (f32[768]{0:T(1024)S(1)}, f32[768]{0:T(1024)}, u32[]{:S(2)}) copy-start(f32[768]{0:T(1024)} %copy-done.11) | copy-start | bytes 9220
  183.5 60.5 %copy-start.14 = (f32[64]{0:T(128)S(1)}, f32[64]{0:T(128)}, u32[]{:S(2)}) copy-start(f32[64]{0:T(128)} %param.17) | copy-start | bytes 772
  244.0 1.0 copy-start.9
  244.0 1.1 copy-start.7
  244.9 1.4 copy-start.2
  248.2 2.5 copy-start.10
  311.3 50.5 %copy-start.3 = (f32[1,768,256]{2,1,0:T(8,128)S(1)}, f32[1,768,256]{2,1,0:T(8,128)}, u32[]{:S(2)}) copy-start(f32[1,768,256]{2,1,0:T(8,128)} %get-tuple-element.40) | copy-start | bytes 2359300
  311.3 50.5 %copy-start.4 = (f32[1,768,256]{2,1,0:T(8,128)S(1)}, f32[1,768,256]{2,1,0:T(8,128)}, u32[]{:S(2)}) copy-start(f32[1,768,256]{2,1,0:T(8,128)} %get-tuple-element.41) | copy-start | bytes 2359300
  311.3 50.5 %copy-start.5 = (f32[1,768,256]{2,1,0:T(8,128)S(1)}, f32[1,768,256]{2,1,0:T(8,128)}, u32[]{:S(2)}) copy-start(f32[1,768,256]{2,1,0:T(8,128)} %get-tuple-element.38) | copy-start | bytes 2359300
Sparse Core Ops, SparseCore 0:
  9.5 51.7 all-gather.6
  63.4 47.6 all-gather.10
  113.3 47.6 all-gather.12
  162.9 73.2 all-gather.14
  238.1 73.1 all-gather.16
  313.2 48.5 all-gather.8
  371.6 57.2 reduce-scatter.1
